TPU v7x, 32 devices: a whole 2x2x4 slice. The times are simulated.
32 devices in a mesh: sp: 8 (over z, y), dp: 4 (over x, core).
Axes of the slice: x: 2, y: 2, z: 4, core: 2. Of those that a mesh axis runs over, the one named last changes fastest.
Arguments:
- query_nope: bfloat16 [4, 2048, 16, 128], P('dp', 'sp'), may hold values from -6 to 6
- query_rope: bfloat16 [4, 2048, 16, 64], P('dp', 'sp'), may hold values from -160 to 160
- latent: bfloat16 [4, 2048, 256], P('dp', 'sp'), may hold values from -6 to 6
- key_rope: bfloat16 [4, 2048, 64], P('dp', 'sp'), may hold values from -4 to 4
- resid: bfloat16 [4, 2048, 2048], P('dp', 'sp'), may hold values from -6 to 6
- latent_gain: float32 [256], replicated, may hold values from 0.1 to 1.9
- key_up: bfloat16 [256, 2048], P(None, 'sp'), may hold values from -0.375 to 0.375
- value_up: bfloat16 [256, 2048], P(None, 'sp'), may hold values from -0.375 to 0.375
- out_proj: bfloat16 [2048, 2048], P('sp', 'dp'), may hold values from -0.125 to 0.125
- norm_gain: float32 [2048], replicated, may hold values from 0.1 to 1.9
- expert_gate: bfloat16 [8, 2048, 1024], P('sp'), may hold values from -0.125 to 0.125
- expert_up: bfloat16 [8, 2048, 1024], P('sp'), may hold values from -0.125 to 0.125
- expert_down: bfloat16 [8, 1024, 2048], P('sp'), may hold values from -0.1875 to 0.1875
- routes: int32 [4, 2048, 2], P('dp', 'sp'), may hold values from 0 to 7, all different within a row; in each aligned block of 256 rows (0 to 255, 256 to 511, ..., all dimensions but the last counted through in order) at most 128 rows name the same one
- route_weight: float32 [4, 2048, 2], P('dp', 'sp'), may hold values from 0.2 to 1
Outputs:
- mixed: bfloat16 [4, 2048, 2048], P('dp', 'sp')
Inputs may be any that keep to these rules, and one draw needn't show every extreme that they name: `routes`: each token names two different experts. Among the tokens of one device no expert is named more than 128 times, and in every draw some expert is named exactly 128 times by some device's tokens.
All inputs are finite; a program needn't handle non-finite values.
Results may differ from a plain program's by a relative error of at most 0.0075.
Values may be sent and summed in bfloat16 or wider, within the bound.
No kernel may reach another device: no remote copies, remote signals or barrier semaphores. Data moves between devices by JAX's collectives and lax.ppermute only.
A program may use at most 128 MiB of HBM per device.

v0:
```python
import jax
import jax.numpy as jnp
from jax import lax
from jax.sharding import PartitionSpec as P

epsilon = 1e-06
rope_base = 10000.0
masked_score = -1e30


def rotate(values, positions):
    half_width = values.shape[-1] // 2
    frequency = rope_base ** (-jnp.arange(half_width, dtype=jnp.float32) / half_width)
    angles = positions.astype(jnp.float32)[:, None] * frequency[None, :]
    cosine = jnp.cos(angles)
    sine_part = jnp.sin(angles)
    if values.ndim == 3:
        cosine = cosine[:, None, :]
        sine_part = sine_part[:, None, :]
    floats = values.astype(jnp.float32)
    first_half = floats[..., :half_width]
    second_half = floats[..., half_width:]
    turned = jnp.concatenate(
        [
            first_half * cosine - second_half * sine_part,
            second_half * cosine + first_half * sine_part,
        ],
        axis=-1,
    )
    return turned.astype(jnp.bfloat16)


def rms_scaled(values, gain):
    floats = values.astype(jnp.float32)
    return floats * lax.rsqrt(jnp.mean(floats * floats, axis=-1, keepdims=True) + epsilon) * gain


def assign_slots(route_block, experts_all, capacity):
    flat_routes = route_block.reshape(-1)
    onehot = (flat_routes[:, None] == jnp.arange(experts_all, dtype=jnp.int32)[None, :]).astype(
        jnp.int32
    )
    earlier = jnp.cumsum(onehot, axis=0) - onehot
    placed = jnp.sum(earlier * onehot, axis=1)
    return flat_routes * capacity + placed


def fill_slots(rows, slot_ids, experts_all, capacity):
    pairs = slot_ids.shape[0]
    matches = jnp.arange(experts_all * capacity, dtype=jnp.int32)[:, None] == slot_ids[None, :]
    source = (
        jnp.sum(jnp.where(matches, jnp.arange(pairs, dtype=jnp.int32)[None, :], 0), axis=1) // 2
    )
    filled = jnp.any(matches, axis=1)
    picked = jnp.take(rows, source, axis=0)
    chosen = jnp.where(filled[:, None], picked, jnp.zeros_like(picked))
    return chosen.reshape(experts_all, capacity, rows.shape[-1])


def combine_slots(returned, slot_ids, weights):
    flat_back = returned.reshape(-1, returned.shape[-1])
    picked = (
        jnp.take(flat_back, slot_ids, axis=0).astype(jnp.float32).reshape(weights.shape[0], 2, -1)
    )
    return jnp.sum(weights[:, :, None] * picked, axis=1)


def shards(
    query_nope,
    query_rope,
    latent,
    key_rope,
    resid,
    latent_gain,
    key_up,
    value_up,
    out_proj,
    norm_gain,
    expert_gate,
    expert_up,
    expert_down,
    routes,
    route_weight,
):
    tokens_here = latent.shape[1]
    sp_count = lax.axis_size("sp")
    length = tokens_here * sp_count
    block = min(512, length)
    blocks = length // block
    local_pos = lax.axis_index("sp") * tokens_here + jnp.arange(tokens_here, dtype=jnp.int32)
    latent_normed = rms_scaled(latent[0], latent_gain).astype(jnp.bfloat16)
    key_turned = rotate(key_rope[0], local_pos)
    query_turned = rotate(query_rope[0], local_pos)
    all_latent, all_keyturn = (
        lax.all_gather(latent_normed, "sp", axis=0, tiled=True),
        lax.all_gather(key_turned, "sp", axis=0, tiled=True),
    )
    query_plain, query_turn = (
        lax.all_to_all(query_nope[0], "sp", split_axis=1, concat_axis=0, tiled=True),
        lax.all_to_all(query_turned, "sp", split_axis=1, concat_axis=0, tiled=True),
    )
    heads_here = query_plain.shape[1]
    key_plain = (
        jnp.dot(all_latent, key_up, preferred_element_type=jnp.float32)
        .astype(jnp.bfloat16)
        .reshape(length, heads_here, -1)
    )
    value_heads = (
        jnp.dot(all_latent, value_up, preferred_element_type=jnp.float32)
        .astype(jnp.bfloat16)
        .reshape(length, heads_here, -1)
    )
    scale = (query_plain.shape[-1] + query_turn.shape[-1]) ** (-0.5)
    key_ids = jnp.arange(length, dtype=jnp.int32)

    def one_block(items):
        index, plain_block, turn_block = items
        scores = jnp.einsum(
            "bhd,shd->hbs", plain_block, key_plain, preferred_element_type=jnp.float32
        )
        scores = (
            scores
            + jnp.einsum("bhr,sr->hbs", turn_block, all_keyturn, preferred_element_type=jnp.float32)
        ) * scale
        row_ids = index * block + jnp.arange(block, dtype=jnp.int32)
        allowed = key_ids[None, :] <= row_ids[:, None]
        scores = jnp.where(allowed[None], scores, masked_score)
        largest = jnp.max(scores, axis=-1, keepdims=True)
        powers = jnp.exp(scores - largest)
        attend = (powers / jnp.sum(powers, axis=-1, keepdims=True)).astype(jnp.bfloat16)
        return jnp.einsum(
            "hbs,shd->bhd", attend, value_heads, preferred_element_type=jnp.float32
        ).astype(jnp.bfloat16)

    attended = lax.map(
        one_block,
        (
            jnp.arange(blocks, dtype=jnp.int32),
            query_plain.reshape(blocks, block, heads_here, -1),
            query_turn.reshape(blocks, block, heads_here, -1),
        ),
    )
    attended = attended.reshape(length, heads_here, -1)
    token_heads = lax.all_to_all(attended, "sp", split_axis=0, concat_axis=1, tiled=True)
    flat_heads = token_heads.reshape(tokens_here, -1)
    head_rows = lax.all_gather(out_proj, "dp", axis=1, tiled=True)
    projected = jnp.dot(
        flat_heads,
        lax.all_gather(head_rows, "sp", axis=0, tiled=True),
        preferred_element_type=jnp.float32,
    ).astype(jnp.bfloat16)
    after_attention = resid[0].astype(jnp.float32) + projected.astype(jnp.float32)
    normed = rms_scaled(after_attention, norm_gain).astype(jnp.bfloat16)
    experts_all = sp_count * expert_gate.shape[0]
    capacity = 4 * tokens_here // experts_all
    slot_ids = assign_slots(routes[0], experts_all, capacity)
    outgoing = fill_slots(normed, slot_ids, experts_all, capacity)
    arrived = lax.all_to_all(outgoing, "sp", split_axis=0, concat_axis=0, tiled=True)
    senders, slots_now, width = arrived.shape
    rows = arrived.reshape(senders * slots_now, width)
    gate = jnp.dot(rows, expert_gate[0], preferred_element_type=jnp.float32)
    upward = jnp.dot(rows, expert_up[0], preferred_element_type=jnp.float32)
    hidden = (jax.nn.silu(gate) * upward).astype(jnp.bfloat16)
    result = jnp.dot(hidden, expert_down[0], preferred_element_type=jnp.float32).astype(
        jnp.bfloat16
    )
    returned = lax.all_to_all(
        result.reshape(senders, slots_now, width), "sp", split_axis=0, concat_axis=0, tiled=True
    )
    routed = combine_slots(returned, slot_ids, route_weight[0])
    return (after_attention + routed).astype(jnp.bfloat16)[None]


def solution(mesh):
    return jax.shard_map(
        shards,
        mesh=mesh,
        in_specs=(
            P("dp", "sp", None, None),
            P("dp", "sp", None, None),
            P("dp", "sp", None),
            P("dp", "sp", None),
            P("dp", "sp", None),
            P(),
            P(None, "sp"),
            P(None, "sp"),
            P("sp", "dp"),
            P(),
            P("sp", None, None),
            P("sp", None, None),
            P("sp", None, None),
            P("dp", "sp", None),
            P("dp", "sp", None),
        ),
        out_specs=P("dp", "sp", None),
        check_vma=False,
    )
```

profile of v0, /device:TPU:0, one launch (start us, length us, event | category | flops | bytes accessed | tf_op | source)
XLA Modules:
  0.0 489.6 jit_solution(9054582442500225814)
XLA Ops:
  12.2 16.1 %all-gather.6.cloned.1.call-done = bf16[256,2048]{1,0:T(8,128)(2,1)} async-done(((bf16[256,512]{1,0:T(8,128)(2,1)}), bf16[256,2048]{1,0:T(8,128)(2,1)}) %all-gather.6.cloned.1.call-update) | async-done | bytes 1048592 | tf_op jit(solution)/shard_map/all_gather | solution.py:146
  29.4 5.5 %all-to-all-start.1 = ((bf16[256,16,64]{0,2,1:T(8,128)(2,1)}), bf16[256,16,64]{0,2,1:T(8,128)(2,1)S(1)}, u32[]{:S(2)}, u32[]{:S(2)}) async-start(bf16[256,16,64]{0,2,1:T(8,128)(2,1)} %pad_maximum_fusion), calls=%async_computation.1 | async-start | bytes 1048576 | tf_op jit(solution)/shard_map/all_to_all | solution.py:100
  36.2 17.7 %all-to-all-done.1 = bf16[256,16,64]{0,2,1:T(8,128)(2,1)S(1)} async-done(((bf16[256,16,64]{0,2,1:T(8,128)(2,1)}), bf16[256,16,64]{0,2,1:T(8,128)(2,1)S(1)}, u32[]{:S(2)}, u32[]{:S(2)}) %all-to-all-start.1) | async-done | bytes 524320 | tf_op jit(solution)/shard_map/all_to_all | solution.py:100
  54.0 3.6 all-to-all-start
  57.6 55.9 %all_gather.13 = bf16[2048,64]{0,1:T(8,128)(2,1)S(1)} all-gather(bf16[256,64]{0,1:T(8,128)(2,1)S(1)} %pad_maximum_fusion.1), channel_id=1, replica_groups=mesh['sp'=8,'dp'=4] {'sp'}, dimensions={0}, use_global_device_ids=true | all-gather | bytes 294912 | tf_op jit(solution)/shard_map/all_gather | solution.py:96
  115.1 2.8 convolution_convert_fusion.1
  119.5 2.4 convolution_convert_fusion
  121.9 2.3 copy.93
  124.3 73.1 %while.11 = (s32[]{:T(128)}, bf16[4,512,2,128]{3,1,0,2:T(8,128)(2,1)}, s32[4]{0:T(128)S(1)}, bf16[4,512,2,128]{3,1,0,2:T(8,128)(2,1)S(1)}, bf16[2048,2,128]{2,0,...) while((s32[]{:T(128)}, ...), condition=%wide.region_4.5_spmd.clone, body=%wide.region_1.4_spmd.clone.sunk | while | flops 1360139776 | bytes 93205688 | solution.py:135
  127.3 2.8 fusion.75
  133.3 9.1 %fusion.77 = bf16[4,512,2,128]{3,1,0,2:T(8,128)(2,1)} fusion(bf16[4,512,2,128]{3,1,0,2:T(8,128)(2,1)} %get-tuple-element.211, s32[]{:T(128)} %get-tuple-element.210, bf16[2048,2,128]{2,0,1:T(8,128)(2,1)S(1)} %copy-done.5, f32[2,512]{1,0:T(2,128)S(1)} %fusion.76, f32[2,512,2048]{2,1,0:T(8,128)} %copy-done.2), kind=kOutput, calls=%fused_computation.13.clone.1 | convolution fusion | flops 543296512 | bytes 18092544 | tf_op jit(solution)/shard_map/while/body/eval_jaxpr/hbs,shd->bhd/dot_general | solution.py:131
  145.5 2.8 fusion.75
  151.5 9.2 %fusion.77 = bf16[4,512,2,128]{3,1,0,2:T(8,128)(2,1)} fusion(bf16[4,512,2,128]{3,1,0,2:T(8,128)(2,1)} %get-tuple-element.211, s32[]{:T(128)} %get-tuple-element.210, bf16[2048,2,128]{2,0,1:T(8,128)(2,1)S(1)} %copy-done.5, f32[2,512]{1,0:T(2,128)S(1)} %fusion.76, f32[2,512,2048]{2,1,0:T(8,128)} %copy-done.2), kind=kOutput, calls=%fused_computation.13.clone.1 | convolution fusion | flops 543296512 | bytes 18092544 | tf_op jit(solution)/shard_map/while/body/eval_jaxpr/hbs,shd->bhd/dot_general | solution.py:131
  163.8 2.8 fusion.75
  169.8 9.1 %fusion.77 = bf16[4,512,2,128]{3,1,0,2:T(8,128)(2,1)} fusion(bf16[4,512,2,128]{3,1,0,2:T(8,128)(2,1)} %get-tuple-element.211, s32[]{:T(128)} %get-tuple-element.210, bf16[2048,2,128]{2,0,1:T(8,128)(2,1)S(1)} %copy-done.5, f32[2,512]{1,0:T(2,128)S(1)} %fusion.76, f32[2,512,2048]{2,1,0:T(8,128)} %copy-done.2), kind=kOutput, calls=%fused_computation.13.clone.1 | convolution fusion | flops 543296512 | bytes 18092544 | tf_op jit(solution)/shard_map/while/body/eval_jaxpr/hbs,shd->bhd/dot_general | solution.py:131
  181.9 2.8 fusion.75
  188.0 9.4 %fusion.77 = bf16[4,512,2,128]{3,1,0,2:T(8,128)(2,1)} fusion(bf16[4,512,2,128]{3,1,0,2:T(8,128)(2,1)} %get-tuple-element.211, s32[]{:T(128)} %get-tuple-element.210, bf16[2048,2,128]{2,0,1:T(8,128)(2,1)S(1)} %copy-done.5, f32[2,512]{1,0:T(2,128)S(1)} %fusion.76, f32[2,512,2048]{2,1,0:T(8,128)} %copy-done.2), kind=kOutput, calls=%fused_computation.13.clone.1 | convolution fusion | flops 543296512 | bytes 18092544 | tf_op jit(solution)/shard_map/while/body/eval_jaxpr/hbs,shd->bhd/dot_general | solution.py:131
  197.3 3.7 copy.95
  201.0 3.7 all-to-all-start.2
  207.4 28.0 %all-to-all-done.2 = bf16[2048,2,128]{2,1,0:T(2,128)(2,1)S(1)} async-done(((bf16[2048,2,128]{2,1,0:T(2,128)(2,1)}), bf16[2048,2,128]{2,1,0:T(2,128)(2,1)S(1)}, u32[]{:S(2)}, u32[]{:S(2)}) %all-to-all-start.2) | async-done | bytes 1048608 | tf_op jit(solution)/shard_map/all_to_all | solution.py:144
  236.2 6.1 %multiply_reduce_fusion.1 = (f32[256]{0:T(256)S(1)}, f32[256,2048]{1,0:T(8,128)S(1)}) fusion(bf16[256,2048]{0,1:T(8,128)(2,1)S(1)} %bitcast.150, bf16[2048,2048]{1,0:T(8,128)(2,1)} %all-gather.8.cloned.1.call-done, bf16[1,256,2048]{2,1,0:T(8,128)(2,1)} %param.21), kind=kOutput, calls=%fused_computation.42 | convolution fusion | flops 2150629120 | bytes 12583936 | tf_op jit(solution)/shard_map/dot_general | solution.py:147
  242.5 6.0 %gather_fusion = bf16[1024,2048]{1,0:T(8,128)(2,1)} fusion(bf16[256,2048]{1,0:T(8,128)(2,1)S(1)} %multiply_convert_fusion.1, s32[1024]{0:T(1024)S(1)} %broadcast_clamp_fusion), kind=kCustom, calls=%fused_computation | custom fusion | bytes 8392704 | tf_op jit(solution)/shard_map/jit(_take)/gather | solution.py:55
  248.5 2.6 select_select_fusion
  251.1 95.5 %all_to_all.55 = bf16[8,128,2048]{2,1,0:T(8,128)(2,1)S(1)} all-to-all(bf16[8,128,2048]{2,1,0:T(8,128)(2,1)S(1)} %select_select_fusion), channel_id=1, replica_groups=mesh['sp'=8,'dp'=4] {'sp'}, dimensions={0} | all-to-all | bytes 8388608 | tf_op jit(solution)/shard_map/all_to_all | solution.py:158
  346.6 4.5 fusion.20
  351.1 5.4 %multiply_convert_fusion = bf16[1024,1024]{1,0:T(8,128)(2,1)S(1)} fusion(f32[1024,1024]{1,0:T(8,128)S(1)} %fusion.20, bf16[1024,2048]{1,0:T(8,128)(2,1)S(1)} %bitcast.154, bf16[1,2048,1024]{2,1,0:T(8,128)(2,1)S(1)} %copy-done.10), kind=kOutput, calls=%fused_computation.31 | convolution fusion | flops 4301258752 | bytes 14680064 | tf_op jit(solution)/shard_map/dot_general | solution.py:161
  356.5 6.1 %fusion.24 = bf16[1024,2048]{1,0:T(8,128)(2,1)} fusion(bf16[1024,1024]{1,0:T(8,128)(2,1)S(1)} %multiply_convert_fusion, bf16[1,1024,2048]{2,1,0:T(8,128)(2,1)S(1)} %copy-done.11), kind=kOutput, calls=%fused_computation.34 | convolution fusion | flops 4297064448 | bytes 10485760 | tf_op jit(solution)/shard_map/dot_general | solution.py:164
  362.6 4.9 all-to-all-start.4
  368.4 91.0 %all-to-all-done.4 = bf16[8,128,2048]{2,1,0:T(8,128)(2,1)} async-done(((bf16[8,128,2048]{2,1,0:T(8,128)(2,1)}), bf16[8,128,2048]{2,1,0:T(8,128)(2,1)}, u32[]{:S(2)}, u32[]{:S(2)}) %all-to-all-start.4) | async-done | bytes 4194336 | tf_op jit(solution)/shard_map/all_to_all | solution.py:167
  459.4 8.0 %gather_fusion.1 = bf16[512,2048]{1,0:T(8,128)(2,1)} fusion(bf16[1024,2048]{1,0:T(8,128)(2,1)} %bitcast.33, s32[1024]{0:T(1024)S(1)} %pad_clamp_fusion), kind=kCustom, calls=%fused_computation.1 | custom fusion | bytes 4196352 | tf_op jit(solution)/shard_map/jit(_take)/gather | solution.py:63
  467.4 4.4 gather.15
  471.9 9.9 %multiply_reduce_fusion = f32[256,2048]{1,0:T(8,128)S(1)} fusion(bf16[256,2,2048]{2,1,0:T(2,128)(2,1)} %gather.15, pred[256,2]{1,0:T(8,128)(4,1)S(1)} %copy.102, f32[256,2]{1,0:T(8,128)S(1)} %copy.98), kind=kLoop, calls=%fused_computation.30 | loop fusion | flops 3670016 | bytes 4196864 | tf_op jit(solution)/shard_map/reduce_sum | solution.py:65
  (114 shorter events, 39.5 us)
Async XLA Ops:
  6.5 108.5 %copy-start = (bf16[256,256]{1,0:T(8,128)(2,1)S(1)}, bf16[256,256]{1,0:T(8,128)(2,1)}, u32[]{:S(2)}) copy-start(bf16[256,256]{1,0:T(8,128)(2,1)} %param.23) | copy-start | bytes 393220
  6.5 28.3 %copy-start.4 = (bf16[1,256,16,128]{3,2,1,0:T(8,128)(2,1)S(1)}, bf16[1,256,16,128]{3,2,1,0:T(8,128)(2,1)}, u32[]{:S(2)}) copy-start(bf16[1,256,16,128]{3,2,1,0:T(8,128)(2,1)} %param.17) | copy-start | bytes 3145732
  6.5 21.8 %all-gather.6.cloned.1.call-start = ((), (), s32[]{:S(2)}) async-start(), calls=%async_computation.6 | async-start | bytes 1310720 | tf_op jit(solution)/shard_map/all_gather | solution.py:146
  7.3 107.8 %all-gather.4.cloned.1.call-start = ((), (), s32[]{:S(2)}) async-start(), calls=%async_computation.5 | async-start | bytes 1179648 | tf_op jit(solution)/shard_map/all_gather | solution.py:95
  10.0 226.1 %all-gather.8.cloned.1.call-start = ((), (), s32[]{:S(2)}) async-start(), calls=%async_computation.7 | async-start | bytes 9437184 | tf_op jit(solution)/shard_map/all_gather | solution.py:149
  29.4 24.6 %all-to-all-start.1 = ((bf16[256,16,64]{0,2,1:T(8,128)(2,1)}), bf16[256,16,64]{0,2,1:T(8,128)(2,1)S(1)}, u32[]{:S(2)}, u32[]{:S(2)}) async-start(bf16[256,16,64]{0,2,1:T(8,128)(2,1)} %pad_maximum_fusion), calls=%async_computation.1 | async-start | bytes 1048576 | tf_op jit(solution)/shard_map/all_to_all | solution.py:100
  54.0 70.2 %all-to-all-start = ((bf16[256,16,128]{2,0,1:T(8,128)(2,1)}), bf16[256,16,128]{2,0,1:T(8,128)(2,1)S(1)}, u32[]{:S(2)}, u32[]{:S(2)}) async-start(bf16[256,16,128]{2,0,1:T(8,128)(2,1)} %bitcast.127), calls=%async_computation | async-start | bytes 2097152 | tf_op jit(solution)/shard_map/all_to_all | solution.py:99
  115.1 4.4 copy-start.3
  130.1 3.2 copy-start.2
  130.1 3.2 copy-start.5
  148.3 3.2 copy-start.2
  148.3 3.2 copy-start.5
  166.5 3.2 copy-start.2
  166.6 3.2 copy-start.5
  184.7 3.2 copy-start.2
  184.7 3.2 copy-start.5
  197.3 7.4 %copy-start.6 = (s32[1,256,2]{1,2,0:T(2,128)S(1)}, s32[1,256,2]{1,2,0:T(2,128)}, u32[]{:S(2)}) copy-start(s32[1,256,2]{1,2,0:T(2,128)} %param.30) | copy-start | bytes 6148
  201.0 34.4 %all-to-all-start.2 = ((bf16[2048,2,128]{2,1,0:T(2,128)(2,1)}), bf16[2048,2,128]{2,1,0:T(2,128)(2,1)S(1)}, u32[]{:S(2)}, u32[]{:S(2)}) async-start(bf16[2048,2,128]{2,1,0:T(2,128)(2,1)} %copy.95), calls=%async_computation.2 | async-start | bytes 2097152 | tf_op jit(solution)/shard_map/all_to_all | solution.py:144
  236.1 6.1 %copy-start.7 = (f32[2048]{0:T(1024)S(1)}, f32[2048]{0:T(1024)}, u32[]{:S(2)}) copy-start(f32[2048]{0:T(1024)} %param.26) | copy-start | bytes 24580
  251.1 95.5 %copy-start.9 = (bf16[1,2048,1024]{2,1,0:T(8,128)(2,1)S(1)}, bf16[1,2048,1024]{2,1,0:T(8,128)(2,1)}, u32[]{:S(2)}) copy-start(bf16[1,2048,1024]{2,1,0:T(8,128)(2,1)} %param.28) | copy-start | bytes 12582916
  346.6 4.5 copy-start.10
  351.1 5.4 %copy-start.11 = (bf16[1,1024,2048]{2,1,0:T(8,128)(2,1)S(1)}, bf16[1,1024,2048]{2,1,0:T(8,128)(2,1)}, u32[]{:S(2)}) copy-start(bf16[1,1024,2048]{2,1,0:T(8,128)(2,1)} %param.29) | copy-start | bytes 12582916
  362.6 5.6 %copy-start.8 = (f32[1,256,2]{1,2,0:T(2,128)S(1)}, f32[1,256,2]{1,2,0:T(2,128)}, u32[]{:S(2)}) copy-start(f32[1,256,2]{1,2,0:T(2,128)} %param.31) | copy-start | bytes 6148
  362.6 96.9 %all-to-all-start.4 = ((bf16[8,128,2048]{2,1,0:T(8,128)(2,1)}), bf16[8,128,2048]{2,1,0:T(8,128)(2,1)}, u32[]{:S(2)}, u32[]{:S(2)}) async-start(bf16[8,128,2048]{2,1,0:T(8,128)(2,1)} %bitcast.152), calls=%async_computation.4 | async-start | bytes 8388608 | tf_op jit(solution)/shard_map/all_to_all | solution.py:167
  467.4 15.6 %copy-start.1 = (bf16[256,256]{1,0:T(8,128)(2,1)S(1)}, bf16[256,256]{1,0:T(8,128)(2,1)}, u32[]{:S(2)}) copy-start(bf16[256,256]{1,0:T(8,128)(2,1)} %param.23) | copy-start | bytes 393220
Sparse Core Ops, SparseCore 0:
  8.9 19.4 all-gather.5
  30.5 57.7 all-gather.3
  90.4 131.3 all-gather.7
where the time goes:
time: 490 us
  waiting for transfers between devices  154 us (31%)
  blocking collectives  151 us (31%)
  matrix products  80.1 us (16%)
  local copies, waits for them, and re-layouts  40 us (8%)
  other arithmetic  30.5 us (6%)
  starting transfers between devices  17.9 us (4%)
  between operations  13.5 us (3%)
    all_to_all x1, blocking collectives, shards(): lax.all_to_all(outgoing, 'sp', split_axis=0, concat_axis=0, tiled=True)  95.5 us
    all_to_all x1, waiting for transfers between devices, shards(): lax.all_to_all(result.reshape(senders, slots_now, width), 'sp', split_axi...  91 us
    all_gather x1, blocking collectives, shards(): lax.all_gather(key_turned, 'sp', axis=0, tiled=True)  55.9 us
    dot_general x4, matrix products, one_block(): jnp.einsum('hbs,shd->bhd', attend, value_heads, preferred_element_type=jn...  36.8 us
    all_to_all x1, waiting for transfers between devices, shards(): lax.all_to_all(attended, 'sp', split_axis=0, concat_axis=1, tiled=True)  28 us
    all_to_all x1, waiting for transfers between devices, shards(): lax.all_to_all(query_turned, 'sp', split_axis=1, concat_axis=0, tiled=True)  17.7 us
    all_gather x1, waiting for transfers between devices, shards(): head_rows = lax.all_gather(out_proj, 'dp', axis=1, tiled=True)  16.1 us
    gather x2, local copies, waits for them, and re-layouts, combine_slots(): jnp.take(flat_back, slot_ids, axis=0).astype(jnp.float32)  12.4 us
  transfers between devices with their start and end apart: 7, of which 4 were waited for; matrix products, arithmetic and copies ran while one was open for 18% of the time, Pallas kernels for 0%

commit v1 on v0

--- a/solution.py
+++ b/solution.py
@@ -141,7 +141,26 @@
         ),
     )
     attended = attended.reshape(length, heads_here, -1)
-    token_heads = lax.all_to_all(attended, "sp", split_axis=0, concat_axis=1, tiled=True)
+
+    def bind_stocks(raw, dev_axis):
+        clean = jax.lax.axis_size(dev_axis)
+        z1, upper = (clean, jax.lax.axis_index(dev_axis))
+        near = raw.shape[0] // z1
+        extra = jnp.roll(raw, shift=-upper * near, axis=0)
+        w_next = lax.slice_in_dim(extra, 0, near, axis=0)
+        src_i = 1
+        arrivals = [w_next]
+        while src_i < z1:
+            all_rows = lax.slice_in_dim(extra, src_i * near, (src_i + 1) * near, axis=0)
+            arrivals.append(
+                jax.lax.ppermute(all_rows, dev_axis, [(rr, (rr + src_i) % z1) for rr in range(z1)])
+            )
+            src_i += 1
+        return jnp.roll(
+            jnp.concatenate(arrivals[::-1], axis=1), (upper + 1) * arrivals[0].shape[1], axis=1
+        )
+
+    token_heads = bind_stocks(attended, "sp")
     flat_heads = token_heads.reshape(tokens_here, -1)
     head_rows = lax.all_gather(out_proj, "dp", axis=1, tiled=True)
     projected = jnp.dot(

time: 490 us -> 482 us (0.984)
  waiting for transfers between devices: 154 us -> 141 us
    ppermute x0 -> x7, waiting for transfers between devices: none -> 38.2 us  [bind_stocks(): jax.lax.ppermute(all_rows, dev_axis, [(rr, (rr + src_i) % z1) for rr in r...]
    all_to_all x1 -> x0, waiting for transfers between devices: 28 us -> none  [shards(): lax.all_to_all(attended, 'sp', split_axis=0, concat_axis=1, tiled=True)]
    all_gather x1, waiting for transfers between devices: 16.1 us -> 4.54 us  [shards(): head_rows = lax.all_gather(out_proj, 'dp', axis=1, tiled=True)]
    all_to_all x1, waiting for transfers between devices: 17.7 us -> 6.58 us  [shards(): lax.all_to_all(query_turned, 'sp', split_axis=1, concat_axis=0, tiled=True)]
    ppermute x0 -> x7, starting transfers between devices: none -> 6.34 us  [bind_stocks(): jax.lax.ppermute(all_rows, dev_axis, [(rr, (rr + src_i) % z1) for rr in r...]
  transfers between devices with their start and end apart: 7 -> 13, of which waited for: 4 -> 8; matrix products, arithmetic and copies ran while one was open for 18% -> 18% of each run, Pallas kernels for 0% -> 0%
where the time goes in v1:
time: 482 us; the launch traced here: 481 us
  blocking collectives  151 us (31%)
  waiting for transfers between devices  141 us (29%)
  matrix products  79.9 us (17%)
  local copies, waits for them, and re-layouts  37.7 us (8%)
  other arithmetic  32.4 us (7%)
  starting transfers between devices  22.3 us (5%)
  between operations  13.7 us (3%)
    all_to_all x1, blocking collectives, shards(): lax.all_to_all(outgoing, 'sp', split_axis=0, concat_axis=0, tiled=True)  95.2 us
    all_to_all x1, waiting for transfers between devices, shards(): lax.all_to_all(result.reshape(senders, slots_now, width), 'sp', split_axi...  91 us
    all_gather x1, blocking collectives, shards(): lax.all_gather(key_turned, 'sp', axis=0, tiled=True)  55.6 us
    ppermute x7, waiting for transfers between devices, bind_stocks(): jax.lax.ppermute(all_rows, dev_axis, [(rr, (rr + src_i) % z1) for rr in r...  38.2 us
    dot_general x4, matrix products, one_block(): jnp.einsum('hbs,shd->bhd', attend, value_heads, preferred_element_type=jn...  36.6 us
    gather x2, local copies, waits for them, and re-layouts, combine_slots(): jnp.take(flat_back, slot_ids, axis=0).astype(jnp.float32)  12.4 us
    dot_general x4, matrix products, one_block(): jnp.einsum('bhr,sr->hbs', turn_block, all_keyturn, preferred_element_type...  11.1 us
    reduce_sum x1, other arithmetic, combine_slots(): return jnp.sum(weights[:, :, None] * picked, axis=1)  9.9 us
  transfers between devices with their start and end apart: 13, of which 8 were waited for; matrix products, arithmetic and copies ran while one was open for 18% of the time, Pallas kernels for 0%

profile of v1, /device:TPU:0, one launch (start us, length us, event | category | flops | bytes accessed | tf_op | source)
XLA Modules:
  0.0 480.6 jit_solution(2635150875767537805)
XLA Ops:
  13.2 7.3 %all-to-all-start.1 = ((bf16[256,16,64]{0,2,1:T(8,128)(2,1)}), bf16[256,16,64]{0,2,1:T(8,128)(2,1)S(1)}, u32[]{:S(2)}, u32[]{:S(2)}) async-start(bf16[256,16,64]{0,2,1:T(8,128)(2,1)} %pad_maximum_fusion), calls=%async_computation.1 | async-start | bytes 1048576 | tf_op jit(solution)/shard_map/all_to_all | solution.py:100
  23.8 4.5 all-gather.6.cloned.1.call-done
  28.5 6.6 %all-to-all-done.1 = bf16[256,16,64]{0,2,1:T(8,128)(2,1)S(1)} async-done(((bf16[256,16,64]{0,2,1:T(8,128)(2,1)}), bf16[256,16,64]{0,2,1:T(8,128)(2,1)S(1)}, u32[]{:S(2)}, u32[]{:S(2)}) %all-to-all-start.1) | async-done | bytes 524320 | tf_op jit(solution)/shard_map/all_to_all | solution.py:100
  35.0 3.6 all-to-all-start
  38.7 55.6 %all_gather.13 = bf16[2048,64]{0,1:T(8,128)(2,1)S(1)} all-gather(bf16[256,64]{0,1:T(8,128)(2,1)S(1)} %pad_maximum_fusion.1), channel_id=1, replica_groups=mesh['sp'=8,'dp'=4] {'sp'}, dimensions={0}, use_global_device_ids=true | all-gather | bytes 294912 | tf_op jit(solution)/shard_map/all_gather | solution.py:96
  96.2 2.8 convolution_convert_fusion.1
  105.4 74.3 %while.11 = (s32[]{:T(128)}, bf16[4,512,2,128]{3,1,0,2:T(8,128)(2,1)}, s32[4]{0:T(128)S(1)}, bf16[4,512,2,128]{3,1,0,2:T(8,128)(2,1)S(1)}, bf16[2048,2,128]{2,0,...) while((s32[]{:T(128)}, ...), condition=%wide.region_4.5_spmd.clone, body=%wide.region_1.4_spmd.clone.sunk | while | flops 1360139776 | bytes 93205688 | solution.py:135
  108.6 2.8 fusion.77
  114.6 9.2 %fusion.79 = bf16[4,512,2,128]{3,1,0,2:T(8,128)(2,1)} fusion(bf16[4,512,2,128]{3,1,0,2:T(8,128)(2,1)} %get-tuple-element.202, s32[]{:T(128)} %get-tuple-element.201, bf16[2048,2,128]{2,0,1:T(8,128)(2,1)S(1)} %copy-done.5, f32[2,512]{1,0:T(2,128)S(1)} %fusion.78, f32[2,512,2048]{2,1,0:T(8,128)} %copy-done.2), kind=kOutput, calls=%fused_computation.13.clone.1 | convolution fusion | flops 543296512 | bytes 18092544 | tf_op jit(solution)/shard_map/while/body/eval_jaxpr/hbs,shd->bhd/dot_general | solution.py:131
  127.0 2.8 fusion.77
  133.8 9.3 %fusion.79 = bf16[4,512,2,128]{3,1,0,2:T(8,128)(2,1)} fusion(bf16[4,512,2,128]{3,1,0,2:T(8,128)(2,1)} %get-tuple-element.202, s32[]{:T(128)} %get-tuple-element.201, bf16[2048,2,128]{2,0,1:T(8,128)(2,1)S(1)} %copy-done.5, f32[2,512]{1,0:T(2,128)S(1)} %fusion.78, f32[2,512,2048]{2,1,0:T(8,128)} %copy-done.2), kind=kOutput, calls=%fused_computation.13.clone.1 | convolution fusion | flops 543296512 | bytes 18092544 | tf_op jit(solution)/shard_map/while/body/eval_jaxpr/hbs,shd->bhd/dot_general | solution.py:131
  146.3 2.8 fusion.77
  152.3 9.1 %fusion.79 = bf16[4,512,2,128]{3,1,0,2:T(8,128)(2,1)} fusion(bf16[4,512,2,128]{3,1,0,2:T(8,128)(2,1)} %get-tuple-element.202, s32[]{:T(128)} %get-tuple-element.201, bf16[2048,2,128]{2,0,1:T(8,128)(2,1)S(1)} %copy-done.5, f32[2,512]{1,0:T(2,128)S(1)} %fusion.78, f32[2,512,2048]{2,1,0:T(8,128)} %copy-done.2), kind=kOutput, calls=%fused_computation.13.clone.1 | convolution fusion | flops 543296512 | bytes 18092544 | tf_op jit(solution)/shard_map/while/body/eval_jaxpr/hbs,shd->bhd/dot_general | solution.py:131
  164.6 2.8 fusion.77
  170.6 9.1 %fusion.79 = bf16[4,512,2,128]{3,1,0,2:T(8,128)(2,1)} fusion(bf16[4,512,2,128]{3,1,0,2:T(8,128)(2,1)} %get-tuple-element.202, s32[]{:T(128)} %get-tuple-element.201, bf16[2048,2,128]{2,0,1:T(8,128)(2,1)S(1)} %copy-done.5, f32[2,512]{1,0:T(2,128)S(1)} %fusion.78, f32[2,512,2048]{2,1,0:T(8,128)} %copy-done.2), kind=kOutput, calls=%fused_computation.13.clone.1 | convolution fusion | flops 543296512 | bytes 18092544 | tf_op jit(solution)/shard_map/while/body/eval_jaxpr/hbs,shd->bhd/dot_general | solution.py:131
  181.6 2.6 collective-permute-start
  184.5 3.0 collective-permute-start.3
  187.7 3.1 collective-permute-done
  190.9 7.0 %collective-permute-done.1 = bf16[256,2,128]{2,0,1:T(8,128)(2,1)S(1)} collective-permute-done((bf16[256,2,128]{2,0,1:T(8,128)(2,1)S(1)}, bf16[256,2,128]{2,0,1:T(8,128)(2,1)S(1)}, u32[]{:S(2)}, u32[]{:S(2)}) %collective-permute-start.1) | collective-permute-done | bytes 131104 | tf_op jit(solution)/shard_map/ppermute | solution.py:156
  198.5 3.6 collective-permute-done.2
  202.1 23.3 %collective-permute-done.3 = bf16[256,2,128]{2,0,1:T(8,128)(2,1)S(1)} collective-permute-done((bf16[256,2,128]{2,0,1:T(8,128)(2,1)S(1)}, bf16[256,2,128]{2,0,1:T(8,128)(2,1)S(1)}, u32[]{:S(2)}, u32[]{:S(2)}) %collective-permute-start.3) | collective-permute-done | bytes 131104 | tf_op jit(solution)/shard_map/ppermute | solution.py:156
  227.6 6.1 %multiply_reduce_fusion.1 = (f32[256]{0:T(256)S(1)}, f32[256,2048]{1,0:T(8,128)S(1)}) fusion(bf16[256,2048]{0,1:T(8,128)(2,1)S(1)} %bitcast.147, bf16[2048,2048]{1,0:T(8,128)(2,1)} %all-gather.8.cloned.1.call-done, bf16[1,256,2048]{2,1,0:T(8,128)(2,1)} %param.21), kind=kOutput, calls=%fused_computation.44 | convolution fusion | flops 2150629120 | bytes 12583936 | tf_op jit(solution)/shard_map/dot_general | solution.py:166
  233.9 6.0 %gather_fusion = bf16[1024,2048]{1,0:T(8,128)(2,1)} fusion(bf16[256,2048]{1,0:T(8,128)(2,1)S(1)} %multiply_convert_fusion.1, s32[1024]{0:T(1024)S(1)} %broadcast_clamp_fusion), kind=kCustom, calls=%fused_computation | custom fusion | bytes 8392704 | tf_op jit(solution)/shard_map/jit(_take)/gather | solution.py:55
  242.5 95.2 %all_to_all.40 = bf16[8,128,2048]{2,1,0:T(8,128)(2,1)S(1)} all-to-all(bf16[8,128,2048]{2,1,0:T(8,128)(2,1)S(1)} %select_select_fusion), channel_id=1, replica_groups=mesh['sp'=8,'dp'=4] {'sp'}, dimensions={0} | all-to-all | bytes 8388608 | tf_op jit(solution)/shard_map/all_to_all | solution.py:177
  337.7 4.5 fusion.20
  342.2 5.4 %multiply_convert_fusion = bf16[1024,1024]{1,0:T(8,128)(2,1)S(1)} fusion(f32[1024,1024]{1,0:T(8,128)S(1)} %fusion.20, bf16[1024,2048]{1,0:T(8,128)(2,1)S(1)} %bitcast.151, bf16[1,2048,1024]{2,1,0:T(8,128)(2,1)S(1)} %copy-done.13), kind=kOutput, calls=%fused_computation.31 | convolution fusion | flops 4301258752 | bytes 14680064 | tf_op jit(solution)/shard_map/dot_general | solution.py:180
  347.6 6.1 %fusion.24 = bf16[1024,2048]{1,0:T(8,128)(2,1)} fusion(bf16[1024,1024]{1,0:T(8,128)(2,1)S(1)} %multiply_convert_fusion, bf16[1,1024,2048]{2,1,0:T(8,128)(2,1)S(1)} %copy-done.14), kind=kOutput, calls=%fused_computation.34 | convolution fusion | flops 4297064448 | bytes 10485760 | tf_op jit(solution)/shard_map/dot_general | solution.py:183
  353.7 4.9 %all-to-all-start.3 = ((bf16[8,128,2048]{2,1,0:T(8,128)(2,1)}), bf16[8,128,2048]{2,1,0:T(8,128)(2,1)}, u32[]{:S(2)}, u32[]{:S(2)}) async-start(bf16[8,128,2048]{2,1,0:T(8,128)(2,1)} %bitcast.149), calls=%async_computation.3 | async-start | bytes 8388608 | tf_op jit(solution)/shard_map/all_to_all | solution.py:186
  359.5 91.0 %all-to-all-done.3 = bf16[8,128,2048]{2,1,0:T(8,128)(2,1)} async-done(((bf16[8,128,2048]{2,1,0:T(8,128)(2,1)}), bf16[8,128,2048]{2,1,0:T(8,128)(2,1)}, u32[]{:S(2)}, u32[]{:S(2)}) %all-to-all-start.3) | async-done | bytes 4194336 | tf_op jit(solution)/shard_map/all_to_all | solution.py:186
  450.5 8.0 %gather_fusion.1 = bf16[512,2048]{1,0:T(8,128)(2,1)} fusion(bf16[1024,2048]{1,0:T(8,128)(2,1)} %bitcast.31, s32[1024]{0:T(1024)S(1)} %pad_clamp_fusion), kind=kCustom, calls=%fused_computation.1 | custom fusion | bytes 4196352 | tf_op jit(solution)/shard_map/jit(_take)/gather | solution.py:63
  458.5 4.4 gather.15
  462.9 9.9 %multiply_reduce_fusion = f32[256,2048]{1,0:T(8,128)S(1)} fusion(bf16[256,2,2048]{2,1,0:T(2,128)(2,1)} %gather.15, pred[256,2]{1,0:T(8,128)(4,1)S(1)} %copy.69, f32[256,2]{1,0:T(8,128)S(1)} %copy.65), kind=kLoop, calls=%fused_computation.30 | loop fusion | flops 3670016 | bytes 4196864 | tf_op jit(solution)/shard_map/reduce_sum | solution.py:65
  (149 shorter events, 51.9 us)
Async XLA Ops:
  6.5 89.7 %copy-start = (bf16[256,256]{1,0:T(8,128)(2,1)S(1)}, bf16[256,256]{1,0:T(8,128)(2,1)}, u32[]{:S(2)}) copy-start(bf16[256,256]{1,0:T(8,128)(2,1)} %param.23) | copy-start | bytes 393220
  6.5 21.8 %all-gather.6.cloned.1.call-start = ((), (), s32[]{:S(2)}) async-start(), calls=%async_computation.5 | async-start | bytes 1310720 | tf_op jit(solution)/shard_map/all_gather | solution.py:165
  7.3 89.0 %all-gather.4.cloned.1.call-start = ((), (), s32[]{:S(2)}) async-start(), calls=%async_computation.4 | async-start | bytes 1179648 | tf_op jit(solution)/shard_map/all_gather | solution.py:95
  12.2 8.4 %copy-start.8 = (s32[1,256,2]{1,2,0:T(2,128)S(1)}, s32[1,256,2]{1,2,0:T(2,128)}, u32[]{:S(2)}) copy-start(s32[1,256,2]{1,2,0:T(2,128)} %param.30) | copy-start | bytes 6148
  12.2 8.9 %copy-start.4 = (bf16[1,256,16,128]{3,2,1,0:T(8,128)(2,1)S(1)}, bf16[1,256,16,128]{3,2,1,0:T(8,128)(2,1)}, u32[]{:S(2)}) copy-start(bf16[1,256,16,128]{3,2,1,0:T(8,128)(2,1)} %param.17) | copy-start | bytes 3145732
  13.2 21.8 %all-to-all-start.1 = ((bf16[256,16,64]{0,2,1:T(8,128)(2,1)}), bf16[256,16,64]{0,2,1:T(8,128)(2,1)S(1)}, u32[]{:S(2)}, u32[]{:S(2)}) async-start(bf16[256,16,64]{0,2,1:T(8,128)(2,1)} %pad_maximum_fusion), calls=%async_computation.1 | async-start | bytes 1048576 | tf_op jit(solution)/shard_map/all_to_all | solution.py:100
  20.6 207.0 %all-gather.8.cloned.1.call-start = ((), (), s32[]{:S(2)}) async-start(), calls=%async_computation.6 | async-start | bytes 9437184 | tf_op jit(solution)/shard_map/all_gather | solution.py:168
  28.5 66.2 %copy-start.6 = (s32[512]{0:T(512)}, s32[512]{0:T(512)S(1)}, u32[]{:S(2)}) copy-start(s32[512]{0:T(512)S(1)} %fusion.38) | copy-start | bytes 6148
  35.0 70.3 %all-to-all-start = ((bf16[256,16,128]{2,0,1:T(8,128)(2,1)}), bf16[256,16,128]{2,0,1:T(8,128)(2,1)S(1)}, u32[]{:S(2)}, u32[]{:S(2)}) async-start(bf16[256,16,128]{2,0,1:T(8,128)(2,1)} %bitcast.124), calls=%async_computation | async-start | bytes 2097152 | tf_op jit(solution)/shard_map/all_to_all | solution.py:99
  96.2 4.4 copy-start.3
  111.4 3.2 copy-start.2
  129.8 4.1 copy-start.2
  129.8 4.1 copy-start.5
  149.1 3.2 copy-start.2
  167.3 3.2 copy-start.2
  167.4 3.2 copy-start.5
  181.6 9.3 %collective-permute-start = (bf16[256,2,128]{2,0,1:T(8,128)(2,1)S(1)}, bf16[256,2,128]{2,0,1:T(8,128)(2,1)S(1)}, u32[]{:S(2)}, u32[]{:S(2)}) collective-permute-start(bf16[256,2,128]{2,0,1:T(8,128)(2,1)S(1)} %get-tuple-element.135), channel_id=1, source_target_pairs={{0,28},{4,0},{8,4},{12,8},{16,12},{20,16},{24,20},{28,24},{1,29},{... | collective-permute-start | bytes 393224 | tf_op jit(solution)/shard_map/ppermute | solution.py:156
  184.2 13.8 %collective-permute-start.1 = (bf16[256,2,128]{2,0,1:T(8,128)(2,1)S(1)}, bf16[256,2,128]{2,0,1:T(8,128)(2,1)S(1)}, u32[]{:S(2)}, u32[]{:S(2)}) collective-permute-start(bf16[256,2,128]{2,0,1:T(8,128)(2,1)S(1)} %get-tuple-element.134), channel_id=1, source_target_pairs={{0,24},{4,28},{8,0},{12,4},{16,8},{20,12},{24,16},{28,20},{1,25},{... | collective-permute-start | bytes 393224 | tf_op jit(solution)/shard_map/ppermute | solution.py:156
  184.5 17.6 %collective-permute-start.2 = (bf16[256,2,128]{2,0,1:T(8,128)(2,1)S(1)}, bf16[256,2,128]{2,0,1:T(8,128)(2,1)S(1)}, u32[]{:S(2)}, u32[]{:S(2)}) collective-permute-start(bf16[256,2,128]{2,0,1:T(8,128)(2,1)S(1)} %get-tuple-element.133), channel_id=1, source_target_pairs={{0,20},{4,24},{8,28},{12,0},{16,4},{20,8},{24,12},{28,16},{1,21},{... | collective-permute-start | bytes 393224 | tf_op jit(solution)/shard_map/ppermute | solution.py:156
  184.5 40.9 %collective-permute-start.3 = (bf16[256,2,128]{2,0,1:T(8,128)(2,1)S(1)}, bf16[256,2,128]{2,0,1:T(8,128)(2,1)S(1)}, u32[]{:S(2)}, u32[]{:S(2)}) collective-permute-start(bf16[256,2,128]{2,0,1:T(8,128)(2,1)S(1)} %get-tuple-element.132), channel_id=1, source_target_pairs={{0,16},{4,20},{8,24},{12,28},{16,0},{20,4},{24,8},{28,12},{1,17},{... | collective-permute-start | bytes 393224 | tf_op jit(solution)/shard_map/ppermute | solution.py:156
  187.5 39.0 %collective-permute-start.4 = (bf16[256,2,128]{2,0,1:T(8,128)(2,1)S(1)}, bf16[256,2,128]{2,0,1:T(8,128)(2,1)S(1)}, u32[]{:S(2)}, u32[]{:S(2)}) collective-permute-start(bf16[256,2,128]{2,0,1:T(8,128)(2,1)S(1)} %get-tuple-element.131), channel_id=1, source_target_pairs={{0,12},{4,16},{8,20},{12,24},{16,28},{20,0},{24,4},{28,8},{1,13},{... | collective-permute-start | bytes 393224 | tf_op jit(solution)/shard_map/ppermute | solution.py:156
  190.9 35.7 %collective-permute-start.5 = (bf16[256,2,128]{2,0,1:T(8,128)(2,1)S(1)}, bf16[256,2,128]{2,0,1:T(8,128)(2,1)S(1)}, u32[]{:S(2)}, u32[]{:S(2)}) collective-permute-start(bf16[256,2,128]{2,0,1:T(8,128)(2,1)S(1)} %get-tuple-element.130), channel_id=1, source_target_pairs={{0,8},{4,12},{8,16},{12,20},{16,24},{20,28},{24,0},{28,4},{1,9},{5... | collective-permute-start | bytes 393224 | tf_op jit(solution)/shard_map/ppermute | solution.py:156
  197.9 28.7 %collective-permute-start.6 = (bf16[256,2,128]{2,0,1:T(8,128)(2,1)S(1)}, bf16[256,2,128]{2,0,1:T(8,128)(2,1)S(1)}, u32[]{:S(2)}, u32[]{:S(2)}) collective-permute-start(bf16[256,2,128]{2,0,1:T(8,128)(2,1)S(1)} %get-tuple-element.129), channel_id=1, source_target_pairs={{0,4},{4,8},{8,12},{12,16},{16,20},{20,24},{24,28},{28,0},{1,5},{5... | collective-permute-start | bytes 393224 | tf_op jit(solution)/shard_map/ppermute | solution.py:156
  227.6 6.1 %copy-start.10 = (f32[2048]{0:T(1024)S(1)}, f32[2048]{0:T(1024)}, u32[]{:S(2)}) copy-start(f32[2048]{0:T(1024)} %param.26) | copy-start | bytes 24580
  242.5 95.2 %copy-start.12 = (bf16[1,2048,1024]{2,1,0:T(8,128)(2,1)S(1)}, bf16[1,2048,1024]{2,1,0:T(8,128)(2,1)}, u32[]{:S(2)}) copy-start(bf16[1,2048,1024]{2,1,0:T(8,128)(2,1)} %param.28) | copy-start | bytes 12582916
  337.7 4.5 copy-start.13
  342.2 5.4 %copy-start.14 = (bf16[1,1024,2048]{2,1,0:T(8,128)(2,1)S(1)}, bf16[1,1024,2048]{2,1,0:T(8,128)(2,1)}, u32[]{:S(2)}) copy-start(bf16[1,1024,2048]{2,1,0:T(8,128)(2,1)} %param.29) | copy-start | bytes 12582916
  353.7 4.9 %copy-start.7 = (s32[512]{0:T(512)S(1)}, s32[512]{0:T(512)}, u32[]{:S(2)}) copy-start(s32[512]{0:T(512)} %copy-done.6) | copy-start | bytes 6148
  353.7 5.1 %copy-start.9 = (s32[1,256,2]{1,2,0:T(2,128)S(1)}, s32[1,256,2]{1,2,0:T(2,128)}, u32[]{:S(2)}) copy-start(s32[1,256,2]{1,2,0:T(2,128)} %param.30) | copy-start | bytes 6148
  353.7 5.7 %copy-start.11 = (f32[1,256,2]{1,2,0:T(2,128)S(1)}, f32[1,256,2]{1,2,0:T(2,128)}, u32[]{:S(2)}) copy-start(f32[1,256,2]{1,2,0:T(2,128)} %param.31) | copy-start | bytes 6148
  353.7 96.9 %all-to-all-start.3 = ((bf16[8,128,2048]{2,1,0:T(8,128)(2,1)}), bf16[8,128,2048]{2,1,0:T(8,128)(2,1)}, u32[]{:S(2)}, u32[]{:S(2)}) async-start(bf16[8,128,2048]{2,1,0:T(8,128)(2,1)} %bitcast.149), calls=%async_computation.3 | async-start | bytes 8388608 | tf_op jit(solution)/shard_map/all_to_all | solution.py:186
  462.9 11.2 %copy-start.1 = (bf16[256,256]{1,0:T(8,128)(2,1)S(1)}, bf16[256,256]{1,0:T(8,128)(2,1)}, u32[]{:S(2)}) copy-start(bf16[256,256]{1,0:T(8,128)(2,1)} %param.23) | copy-start | bytes 393220
  (2 other events, 6.4 us)
Sparse Core Ops, SparseCore 0:
  8.9 19.4 all-gather.5
  30.5 49.5 all-gather.3
  82.2 143.7 all-gather.7
